TPU v7x, 32 devices: a whole 2x2x4 slice. The times are simulated.
32 devices in a mesh: ep: 8 (over z, x), tp: 4 (over y, core).
Axes of the slice: x: 2, y: 2, z: 4, core: 2. Of those that a mesh axis runs over, the one named last changes fastest.
Arguments:
- tokens: bfloat16 [32, 2048], P('ep'), may hold values from -6 to 6
- norm_gain: bfloat16 [2048], replicated, may hold values from 0.099609375 to 1.8984375
- in_weight: bfloat16 [2048, 1024], P(None, 'tp'), may hold values from -0.125 to 0.125
- decay_rate: float32 [64, 64], P('tp'), may hold values from 0.05 to 1
- frequency: float32 [64, 64], P('tp'), may hold values from -3 to 3
- log_step: float32 [64], P('tp'), may hold values from -2.3 to 0.7
- input_real: float32 [64, 64, 16], P('tp'), may hold values from -1.75 to 1.75
- input_imag: float32 [64, 64, 16], P('tp'), may hold values from -1.75 to 1.75
- output_real: float32 [64, 16, 64], P('tp'), may hold values from -0.5 to 0.5
- output_imag: float32 [64, 16, 64], P('tp'), may hold values from -0.5 to 0.5
- skip_gain: float32 [1024], P('tp'), may hold values from -3 to 3
- state_real: float32 [32, 64, 64], P('ep', 'tp'), may hold values from -6 to 6
- state_imag: float32 [32, 64, 64], P('ep', 'tp'), may hold values from -6 to 6
- out_weight: bfloat16 [1024, 2048], P('tp'), may hold values from -0.1875 to 0.1875
- ffn_gain: bfloat16 [2048], replicated, may hold values from 0.099609375 to 1.8984375
- expert_ids: int32 [32, 2], replicated, may hold values from 0 to 7, all different within a row; in each aligned block of 4 rows (0 to 3, 4 to 7, ...) at most 2 rows name the same one
- route_weights: float32 [32, 2], P('ep'), may hold values from 0.2 to 1
- gate_weight: bfloat16 [2048, 65536], P(None, ('ep', 'tp')), may hold values from -0.125 to 0.125
- up_weight: bfloat16 [2048, 65536], P(None, ('ep', 'tp')), may hold values from -0.125 to 0.125
- down_weight: bfloat16 [65536, 2048], P('ep', 'tp'), may hold values from -0.0625 to 0.0625
Outputs:
- mixed: bfloat16 [32, 2048], P('ep', 'tp')
- new_real: float32 [32, 64, 64], P('ep', 'tp')
- new_imag: float32 [32, 64, 64], P('ep', 'tp')
Inputs may be any that keep to these rules, and one draw needn't show every extreme that they name: `expert_ids`: the 2 experts of a row differ. In each aligned block of 4 rows (the rows of one index of ep) no expert is named by more than 2 rows, and in some blocks one expert is named by exactly 2 rows.
All inputs are finite; a program needn't handle non-finite values.
Results may differ from a plain program's by a relative error of at most 0.007.
Values may be sent and summed in bfloat16 or wider, within the bound.
A program may use at most 64 MiB of HBM per device.

v0:
```python
import jax
import jax.numpy as jnp
from jax import lax
from jax.sharding import PartitionSpec as P

EXPERTS = 8
EPSILON = 1e-06


def rms_scale(values, gain):
    floats = values.astype(jnp.float32)
    return (
        floats
        * lax.rsqrt(jnp.mean(floats * floats, axis=-1, keepdims=True) + EPSILON)
        * gain.astype(jnp.float32)
    )


def discretize(decay_rate, frequency, log_step, input_real, input_imag):
    step_size = jnp.exp(log_step)[:, None]
    lam_real = -decay_rate
    magnitude = jnp.exp(lam_real * step_size)
    turned = frequency * step_size
    bar_real = magnitude * jnp.cos(turned)
    bar_imag = magnitude * jnp.sin(turned)
    denom = lam_real * lam_real + frequency * frequency
    minus_one = bar_real - 1.0
    factor_real = (minus_one * lam_real + bar_imag * frequency) / denom
    factor_imag = (bar_imag * lam_real - minus_one * frequency) / denom
    b_real = factor_real[..., None] * input_real - factor_imag[..., None] * input_imag
    b_imag = factor_real[..., None] * input_imag + factor_imag[..., None] * input_real
    return (bar_real, bar_imag, b_real, b_imag)


def state_update(
    projected,
    state_real,
    state_imag,
    decay_rate,
    frequency,
    log_step,
    input_real,
    input_imag,
    output_real,
    output_imag,
    skip_gain,
):
    bar_real, bar_imag, b_real, b_imag = discretize(
        decay_rate, frequency, log_step, input_real, input_imag
    )
    count, groups, _ = state_real.shape
    high = lax.Precision.HIGHEST
    grouped = projected.astype(jnp.float32).reshape(count, groups, -1)
    drive_real = jnp.einsum("sgp,gnp->sgn", grouped, b_real, precision=high)
    drive_imag = jnp.einsum("sgp,gnp->sgn", grouped, b_imag, precision=high)
    new_real = bar_real * state_real - bar_imag * state_imag + drive_real
    new_imag = bar_real * state_imag + bar_imag * state_real + drive_imag
    readout = jnp.einsum("sgn,gpn->sgp", new_real, output_real, precision=high) - jnp.einsum(
        "sgn,gpn->sgp", new_imag, output_imag, precision=high
    )
    readout = readout.reshape(count, -1) + skip_gain * grouped.reshape(count, -1)
    return (jax.nn.gelu(readout).astype(jnp.bfloat16), new_real, new_imag)


def slot_table(own_ids, own_weights, slot_count):
    expert_range = jnp.arange(EXPERTS, dtype=jnp.int32)
    onehot = (own_ids[:, :, None] == expert_range).astype(jnp.int32)
    flat = onehot.reshape(-1, EXPERTS)
    before = (jnp.cumsum(flat, axis=0) - flat).reshape(onehot.shape)
    slots = jnp.arange(slot_count, dtype=jnp.int32)
    match = (before[..., None] == slots) & (onehot[..., None] > 0)
    table = jnp.sum(jnp.where(match, own_weights[:, :, None, None], 0.0), axis=1)
    return jnp.transpose(table, (1, 2, 0))


def shards(
    tokens,
    norm_gain,
    in_weight,
    decay_rate,
    frequency,
    log_step,
    input_real,
    input_imag,
    output_real,
    output_imag,
    skip_gain,
    state_real,
    state_imag,
    out_weight,
    ffn_gain,
    expert_ids,
    route_weights,
    gate_weight,
    up_weight,
    down_weight,
):
    normed_in = rms_scale(tokens, norm_gain).astype(jnp.bfloat16)
    projected = jnp.dot(normed_in, in_weight, preferred_element_type=jnp.float32).astype(
        jnp.bfloat16
    )
    activated, new_real, new_imag = state_update(
        projected,
        state_real,
        state_imag,
        decay_rate,
        frequency,
        log_step,
        input_real,
        input_imag,
        output_real,
        output_imag,
        skip_gain,
    )
    delta = lax.psum(jnp.dot(activated, out_weight, preferred_element_type=jnp.float32), "tp")
    hidden_state = (tokens.astype(jnp.float32) + delta).astype(jnp.bfloat16)
    normed = rms_scale(hidden_state, ffn_gain).astype(jnp.bfloat16)
    seq_count, width = normed.shape
    slot_count = seq_count // 2
    group_span = lax.axis_size("ep") // EXPERTS
    my_index = lax.axis_index("ep")
    own_ids = lax.dynamic_slice_in_dim(expert_ids, my_index * seq_count, seq_count, 0)
    unit_weights = jnp.ones(own_ids.shape, jnp.float32)
    select = slot_table(own_ids, unit_weights, slot_count)
    outgoing = jnp.einsum(
        "xcs,sd->xcd", select.astype(jnp.bfloat16), normed, preferred_element_type=jnp.float32
    ).astype(jnp.bfloat16)
    received = lax.all_to_all(
        jnp.repeat(outgoing, group_span, axis=0), "ep", split_axis=0, concat_axis=0, tiled=True
    )
    slot_rows = received.reshape(-1, width)
    gate_pre = jnp.dot(slot_rows, gate_weight, preferred_element_type=jnp.float32)
    up_pre = jnp.dot(slot_rows, up_weight, preferred_element_type=jnp.float32)
    hidden = (jax.nn.silu(gate_pre) * up_pre).astype(jnp.bfloat16)
    quarter = down_weight.shape[1]
    partial_out = jnp.dot(
        lax.all_gather(hidden, "tp", axis=1, tiled=True),
        down_weight,
        preferred_element_type=jnp.float32,
    )
    rounded = partial_out.astype(jnp.bfloat16).reshape(-1, slot_count, quarter)
    returned = lax.all_to_all(rounded, "ep", split_axis=0, concat_axis=0, tiled=True)
    summed = (
        returned.astype(jnp.float32).reshape(EXPERTS, group_span, slot_count, quarter).sum(axis=1)
    )
    weight_table = slot_table(own_ids, route_weights, slot_count)
    routed = jnp.einsum("xcs,xcd->sd", weight_table, summed, precision=lax.Precision.HIGHEST)
    residual = lax.dynamic_slice_in_dim(hidden_state, lax.axis_index("tp") * quarter, quarter, 1)
    mixed = (residual.astype(jnp.float32) + routed).astype(jnp.bfloat16)
    return (mixed, new_real, new_imag)


def solution(mesh):
    in_specs = (
        P("ep", None),
        P(),
        P(None, "tp"),
        P("tp", None),
        P("tp", None),
        P("tp"),
        P("tp", None, None),
        P("tp", None, None),
        P("tp", None, None),
        P("tp", None, None),
        P("tp"),
        P("ep", "tp", None),
        P("ep", "tp", None),
        P("tp", None),
        P(),
        P(),
        P("ep", None),
        P(None, ("ep", "tp")),
        P(None, ("ep", "tp")),
        P("ep", "tp"),
    )
    out_specs = (P("ep", "tp"), P("ep", "tp", None), P("ep", "tp", None))
    return jax.shard_map(shards, mesh=mesh, in_specs=in_specs, out_specs=out_specs, check_vma=False)
```

profile of v0, /device:TPU:0, one launch (start us, length us, event | category | flops | bytes accessed | tf_op | source)
XLA Modules:
  0.0 71.3 jit_solution(13652618909060821899)
XLA Ops:
  0.7 0.8 %constant_dynamic-slice_fusion = s32[4,2]{0,1:T(2,128)S(1)} fusion(s32[32,2]{0,1:T(2,128)} %param.35, s32[]{:T(128)S(6)} %select_n.14), kind=kLoop, calls=%fused_computation.78 | loop fusion | bytes 68 | tf_op jit(solution)/shard_map/dynamic_slice | solution.py:122
  1.7 0.7 exp.10
  2.4 0.9 %fusion.19 = f32[4]{0:T(128)S(1)} fusion(bf16[4,2048]{1,0:T(4,128)(2,1)} %param.20), kind=kLoop, calls=%fused_computation.32 | loop fusion | flops 24572 | bytes 16400 | tf_op jit(solution)/shard_map/reduce_sum | solution.py:14
  3.3 0.7 convert_element_type.68
  4.0 1.5 %convolution_convert_fusion.2 = bf16[4,256]{1,0:T(4,128)(2,1)S(1)} fusion(bf16[2048,256]{1,0:T(8,128)(2,1)} %param.22, bf16[4,2048]{1,0:T(4,128)(2,1)} %param.20, f32[2048]{0:T(1024)S(1)} %convert_element_type.68, f32[4]{0:T(128)S(1)} %add_rsqrt_fusion.1), kind=kOutput, calls=%fused_computation.13 | convolution fusion | flops 4228096 | bytes 1075216 | tf_op jit(solution)/shard_map/dot_general | solution.py:99
  5.6 0.8 %cosine_multiply_fusion = (f32[16,64]{1,0:T(8,128)S(1)}, f32[16,64]{1,0:T(8,128)S(1)}, f32[16,64]{1,0:T(8,128)S(1)}, f32[16,64]{1,0:T(8,128)S(1)}) fusion(f32[16,64]{1,0:T(8,128)} %param.24, f32[16,64]{1,0:T(8,128)} %param.23, f32[16]{0:T(128)S(1)} %exp.10), kind=kLoop, calls=%fused_computation.51 | loop fusion | flops 17408 | bytes 24640 | tf_op jit(solution)/shard_map/mul | solution.py:24
  6.4 1.2 %fusion.2 = f32[4,16,64]{2,0,1:T(4,128)S(1)} fusion(f32[16,64,16]{1,2,0:T(8,128)} %param.26, f32[16,64,16]{1,2,0:T(8,128)} %param.27, f32[16,64]{1,0:T(8,128)S(1)} %get-tuple-element.21, f32[16,64]{1,0:T(8,128)S(1)} %get-tuple-element.20, f32[4,16,64]{2,1,0:T(8,128)} %param.32, f32[4,16,64]{2,1,0:T(8,128)} %param.31, f32[16,64]{1,0:T(8,128)S(1)} %get-tuple-element.22, ...), kind=kOutput, calls=%fused_computation.6 | convolution fusion | flops 851968 | bytes 198656 | tf_op jit(solution)/shard_map/sgp,gnp->sgn/dot_general | solution.py:55
  7.6 1.2 %fusion.3 = f32[4,16,64]{2,0,1:T(4,128)S(1)} fusion(f32[16,64,16]{1,2,0:T(8,128)} %param.27, f32[16,64,16]{1,2,0:T(8,128)} %param.26, f32[16,64]{1,0:T(8,128)S(1)} %get-tuple-element.21, f32[16,64]{1,0:T(8,128)S(1)} %get-tuple-element.20, f32[4,16,64]{2,1,0:T(8,128)} %param.32, f32[4,16,64]{2,1,0:T(8,128)} %param.31, f32[16,64]{1,0:T(8,128)S(1)} %get-tuple-element.22, ...), kind=kOutput, calls=%fused_computation.8 | convolution fusion | flops 851968 | bytes 198656 | tf_op jit(solution)/shard_map/sgp,gnp->sgn/dot_general | solution.py:54
  9.0 0.7 convert_element_type.80
  9.7 1.2 %fusion.60 = f32[16,4,16]{2,1,0:T(4,128)S(1)} fusion(f32[4,16,64]{2,0,1:T(4,128)S(1)} %fusion.3, f32[16,16,64]{2,1,0:T(8,128)} %param.28), kind=kOutput, calls=%fused_computation.84 | convolution fusion | flops 786432 | bytes 86016 | tf_op jit(solution)/shard_map/sgn,gpn->sgp/dot_general | solution.py:58
  10.9 1.2 %fusion.1 = f32[4,16,16]{2,0,1:T(4,128)S(1)} fusion(f32[16,4,16]{2,1,0:T(4,128)S(1)} %fusion.60, f32[4,16,64]{2,0,1:T(4,128)S(1)} %fusion.2, f32[16,16,64]{2,1,0:T(8,128)} %param.29), kind=kOutput, calls=%fused_computation.4 | convolution fusion | flops 787456 | bytes 90112 | tf_op jit(solution)/shard_map/sgn,gpn->sgp/dot_general | solution.py:58
  12.2 0.9 %fusion.46 = f32[4,2048]{1,0:T(4,128)S(1)} fusion(bf16[256,2048]{1,0:T(8,128)(2,1)S(1)} %copy-done, f32[4,256]{1,0:T(4,128)S(1)} %reshape.73, bf16[4,256]{1,0:T(4,128)(2,1)S(1)} %convolution_convert_fusion.2, f32[256]{0:T(256)} %param.30), kind=kOutput, calls=%fused_computation.69 | convolution fusion | flops 4206592 | bytes 1088512 | tf_op jit(solution)/shard_map/dot_general | solution.py:115
  13.2 12.9 %psum.7 = f32[4,2048]{1,0:T(4,128)S(1)} all-reduce(f32[4,2048]{1,0:T(4,128)S(1)} %fusion.46), channel_id=1, replica_groups=mesh['ep'=8,'tp'=4] {'tp'}, use_global_device_ids=true, to_apply=%region_1.0 | all-reduce | flops 8192 | bytes 65536 | tf_op jit(solution)/shard_map/psum | solution.py:115
  26.1 0.9 %fusion.16 = (f32[4]{0:T(128)S(1)}, bf16[4,2048]{1,0:T(4,128)(2,1)S(1)}) fusion(f32[4,2048]{1,0:T(4,128)S(1)} %psum.7, bf16[4,2048]{1,0:T(4,128)(2,1)} %param.20), kind=kLoop, calls=%fused_computation.29 | loop fusion | flops 49148 | bytes 65552 | tf_op jit(solution)/shard_map/reduce_sum | solution.py:14
  26.9 0.8 %select_reduce_fusion.1 = (f32[4,8,2]{1,0,2:T(4,128)S(1)}, bf16[4,8,2]{1,0,2:T(4,128)(2,1)S(1)}) fusion(f32[4,2]{0,1:T(2,128)} %param.36, s32[4,2,8]{2,0,1:T(4,128)S(1)} %copy.73, pred[4,2,8]{2,0,1:T(4,128)(4,1)S(1)} %copy.74), kind=kLoop, calls=%fused_computation.45 | loop fusion | flops 640 | bytes 736 | tf_op jit(solution)/shard_map/reduce_sum | solution.py:72
  28.0 12.5 %all_to_all.10 = bf16[8,2,2048]{2,1,0:T(2,128)(2,1)S(1)} all-to-all(bf16[8,2,2048]{2,1,0:T(2,128)(2,1)S(1)} %copy.75), channel_id=1, replica_groups=mesh['ep'=8,'tp'=4] {'ep'}, dimensions={0} | all-to-all | bytes 131072 | tf_op jit(solution)/shard_map/all_to_all | solution.py:128
  40.5 4.6 %fusion.61 = f32[16,2048]{1,0:T(8,128)S(1)} fusion(bf16[16,2048]{1,0:T(8,128)(2,1)S(1)} %reshape.74, bf16[2048,2048]{1,0:T(8,128)(2,1)} %param.37), kind=kOutput, calls=%fused_computation.85 | convolution fusion | flops 134217728 | bytes 8585216 | tf_op jit(solution)/shard_map/dot_general | solution.py:132
  45.1 4.6 %fusion = bf16[16,2048]{1,0:T(8,128)(2,1)S(1)} fusion(bf16[16,2048]{1,0:T(8,128)(2,1)S(1)} %reshape.74, bf16[2048,2048]{1,0:T(8,128)(2,1)} %param.38, f32[16,2048]{1,0:T(8,128)S(1)} %fusion.61), kind=kOutput, calls=%fused_computation.2 | convolution fusion | flops 134414336 | bytes 8650752 | tf_op jit(solution)/shard_map/dot_general | solution.py:133
  49.7 5.8 %all_gather.3 = bf16[16,8192]{1,0:T(8,128)(2,1)S(1)} all-gather(bf16[16,2048]{1,0:T(8,128)(2,1)S(1)} %fusion), channel_id=1, replica_groups=mesh['ep'=8,'tp'=4] {'tp'}, dimensions={1}, use_global_device_ids=true | all-gather | bytes 327680 | tf_op jit(solution)/shard_map/all_gather | solution.py:137
  55.5 4.6 %convolution_convert_fusion.1 = bf16[16,512]{1,0:T(8,128)(2,1)S(1)} fusion(bf16[16,8192]{1,0:T(8,128)(2,1)S(1)} %all_gather.3, bf16[8192,512]{1,0:T(8,128)(2,1)} %param.39), kind=kOutput, calls=%fused_computation.9 | convolution fusion | flops 134225920 | bytes 8667136 | tf_op jit(solution)/shard_map/dot_general | solution.py:136
  60.0 0.6 reshape.75
  60.7 3.3 %all-to-all-start.1 = ((bf16[8,2,512]{2,1,0:T(2,128)(2,1)}), bf16[8,2,512]{2,1,0:T(2,128)(2,1)S(1)}, u32[]{:S(2)}, u32[]{:S(2)}) async-start(bf16[8,2,512]{2,1,0:T(2,128)(2,1)} %reshape.75), calls=%async_computation.1 | async-start | bytes 32768 | tf_op jit(solution)/shard_map/all_to_all | solution.py:142
  65.2 5.3 %all-to-all-done.1 = bf16[8,2,512]{2,1,0:T(2,128)(2,1)S(1)} async-done(((bf16[8,2,512]{2,1,0:T(2,128)(2,1)}), bf16[8,2,512]{2,1,0:T(2,128)(2,1)S(1)}, u32[]{:S(2)}, u32[]{:S(2)}) %all-to-all-start.1) | async-done | bytes 16416 | tf_op jit(solution)/shard_map/all_to_all | solution.py:142
  70.5 0.8 %fusion.5 = bf16[4,512]{1,0:T(4,128)(2,1)} fusion(bf16[8,2,512]{2,1,0:T(2,128)(2,1)S(1)} %all-to-all-done.1, f32[4,8,2]{1,0,2:T(4,128)S(1)} %get-tuple-element.15, bf16[4,2048]{1,0:T(4,128)(2,1)S(1)} %get-tuple-element.18, s32[]{:T(128)S(6)} %select_n.13), kind=kOutput, calls=%fused_computation.12 | convolution fusion | flops 399360 | bytes 24836 | tf_op jit(solution)/shard_map/xcs,xcd->sd/dot_general | solution.py:147
  (20 shorter events, 2.2 us)
Async XLA Ops:
  0.6 11.6 %copy-start = (bf16[256,2048]{1,0:T(8,128)(2,1)S(1)}, bf16[256,2048]{1,0:T(8,128)(2,1)}, u32[]{:S(2)}) copy-start(bf16[256,2048]{1,0:T(8,128)(2,1)} %param.33) | copy-start | bytes 3145732
  60.7 9.9 %all-to-all-start.1 = ((bf16[8,2,512]{2,1,0:T(2,128)(2,1)}), bf16[8,2,512]{2,1,0:T(2,128)(2,1)S(1)}, u32[]{:S(2)}, u32[]{:S(2)}) async-start(bf16[8,2,512]{2,1,0:T(2,128)(2,1)} %reshape.75), calls=%async_computation.1 | async-start | bytes 32768 | tf_op jit(solution)/shard_map/all_to_all | solution.py:142
where the time goes:
time: 72.1 us; the launch traced here: 71.3 us
  blocking collectives  31.2 us (43%)
  matrix products  22 us (31%)
  waiting for transfers between devices  5.28 us (7%)
  other arithmetic  4.97 us (7%)
  local copies, waits for them, and re-layouts  3.84 us (5%)
  starting transfers between devices  3.33 us (5%)
  between operations  0.73 us (1%)
    psum x1, blocking collectives, shards(): lax.psum(jnp.dot(activated, out_weight, preferred_element_type=jnp.float3...  12.9 us
    all_to_all x1, blocking collectives, shards(): lax.all_to_all(jnp.repeat(outgoing, group_span, axis=0), 'ep', split_axis...  12.5 us
    all_gather x1, blocking collectives, shards(): lax.all_gather(hidden, 'tp', axis=1, tiled=True)  5.77 us
    all_to_all x1, waiting for transfers between devices, shards(): lax.all_to_all(rounded, 'ep', split_axis=0, concat_axis=0, tiled=True)  5.28 us
    dot_general x1, matrix products, shards(): up_pre = jnp.dot(slot_rows, up_weight, preferred_element_type=jnp.float32)  4.58 us
    dot_general x1, matrix products, shards(): jnp.dot(slot_rows, gate_weight, preferred_element_type=jnp.float32)  4.58 us
    dot_general x1, matrix products, shards(): jnp.dot(lax.all_gather(hidden, 'tp', axis=1, tiled=True), down_weight, pr...  4.56 us
    all_to_all x1, starting transfers between devices, shards(): lax.all_to_all(rounded, 'ep', split_axis=0, concat_axis=0, tiled=True)  3.33 us
  transfers between devices with their start and end apart: 1, of which 1 were waited for; matrix products, arithmetic and copies ran while one was open for 2% of the time, Pallas kernels for 0%

commit v1 on v0

--- a/solution.py
+++ b/solution.py
@@ -134,7 +134,9 @@
     hidden = (jax.nn.silu(gate_pre) * up_pre).astype(jnp.bfloat16)
     quarter = down_weight.shape[1]
     partial_out = jnp.dot(
-        lax.all_gather(hidden, "tp", axis=1, tiled=True),
+        jnp.concatenate(
+            lax.all_to_all(jnp.stack([hidden] * lax.axis_size("tp")), "tp", 0, 0), axis=1
+        ),
         down_weight,
         preferred_element_type=jnp.float32,
     )

time: 72.1 us -> 69.4 us (0.963)
  matrix products: 22 us -> 15.4 us
  blocking collectives: 31.2 us -> 33.9 us
  local copies, waits for them, and re-layouts: 3.84 us -> 4.92 us
    all_to_all x0 -> x1, blocking collectives: none -> 8.52 us  [shards(): lax.all_to_all(jnp.stack([hidden] * lax.axis_size('tp')), 'tp', 0, 0)]
    all_gather x1 -> x0, blocking collectives: 5.77 us -> none  [shards(): lax.all_gather(hidden, 'tp', axis=1, tiled=True)]
    dot_general x1, matrix products: 4.58 us -> 1.2 us  [shards(): up_pre = jnp.dot(slot_rows, up_weight, preferred_element_type=jnp.float32)]
    dot_general x1, matrix products: 4.56 us -> 1.18 us  [shards(): jnp.dot(jnp.concatenate(lax.all_to_all(jnp.stack([hidden] * lax.axis_size...]
    unnamed x4 -> x10, local copies, waits for them, and re-layouts: 1.24 us -> 2.28 us
where the time goes in v1:
time: 69.4 us; the launch traced here: 68.6 us
  blocking collectives  33.9 us (49%)
  matrix products  15.4 us (22%)
  waiting for transfers between devices  5.28 us (8%)
  other arithmetic  4.97 us (7%)
  local copies, waits for them, and re-layouts  4.92 us (7%)
  starting transfers between devices  3.33 us (5%)
  between operations  0.78 us (1%)
    psum x1, blocking collectives, shards(): lax.psum(jnp.dot(activated, out_weight, preferred_element_type=jnp.float3...  12.9 us
    all_to_all x1, blocking collectives, shards(): lax.all_to_all(jnp.repeat(outgoing, group_span, axis=0), 'ep', split_axis...  12.5 us
    all_to_all x1, blocking collectives, shards(): lax.all_to_all(jnp.stack([hidden] * lax.axis_size('tp')), 'tp', 0, 0)  8.52 us
    all_to_all x1, waiting for transfers between devices, shards(): lax.all_to_all(rounded, 'ep', split_axis=0, concat_axis=0, tiled=True)  5.28 us
    dot_general x1, matrix products, shards(): jnp.dot(slot_rows, gate_weight, preferred_element_type=jnp.float32)  4.73 us
    all_to_all x1, starting transfers between devices, shards(): lax.all_to_all(rounded, 'ep', split_axis=0, concat_axis=0, tiled=True)  3.33 us
    unnamed x10, local copies, waits for them, and re-layouts  2.28 us
    reduce_sum x2, other arithmetic, rms_scale(): jnp.mean(floats * floats, axis=-1, keepdims=True) + EPSILON  1.7 us
  transfers between devices with their start and end apart: 1, of which 1 were waited for; matrix products, arithmetic and copies ran while one was open for 2% of the time, Pallas kernels for 0%

profile of v1, /device:TPU:0, one launch (start us, length us, event | category | flops | bytes accessed | tf_op | source)
XLA Modules:
  0.0 68.6 jit_solution(2072003594796778317)
XLA Ops:
  0.7 0.8 %constant_dynamic-slice_fusion = s32[4,2]{0,1:T(2,128)S(1)} fusion(s32[32,2]{0,1:T(2,128)} %param.35, s32[]{:T(128)S(6)} %select_n.14), kind=kLoop, calls=%fused_computation.78 | loop fusion | bytes 68 | tf_op jit(solution)/shard_map/dynamic_slice | solution.py:122
  1.7 0.7 exp.10
  2.4 0.9 %fusion.19 = f32[4]{0:T(128)S(1)} fusion(bf16[4,2048]{1,0:T(4,128)(2,1)} %param.20), kind=kLoop, calls=%fused_computation.32 | loop fusion | flops 24572 | bytes 16400 | tf_op jit(solution)/shard_map/reduce_sum | solution.py:14
  3.3 0.7 %convert_element_type.68 = f32[2048]{0:T(1024)S(1)} convert(bf16[2048]{0:T(1024)(128)(2,1)} %param.21) | non-fusion elementwise | flops 2048 | bytes 12288 | tf_op jit(solution)/shard_map/convert_element_type | solution.py:15
  4.0 1.5 %convolution_convert_fusion.2 = bf16[4,256]{1,0:T(4,128)(2,1)S(1)} fusion(bf16[2048,256]{1,0:T(8,128)(2,1)} %param.22, bf16[4,2048]{1,0:T(4,128)(2,1)} %param.20, f32[2048]{0:T(1024)S(1)} %convert_element_type.68, f32[4]{0:T(128)S(1)} %add_rsqrt_fusion.1), kind=kOutput, calls=%fused_computation.13 | convolution fusion | flops 4228096 | bytes 1075216 | tf_op jit(solution)/shard_map/dot_general | solution.py:99
  5.6 0.8 %cosine_multiply_fusion = (f32[16,64]{1,0:T(8,128)S(1)}, f32[16,64]{1,0:T(8,128)S(1)}, f32[16,64]{1,0:T(8,128)S(1)}, f32[16,64]{1,0:T(8,128)S(1)}) fusion(f32[16,64]{1,0:T(8,128)} %param.24, f32[16,64]{1,0:T(8,128)} %param.23, f32[16]{0:T(128)S(1)} %exp.10), kind=kLoop, calls=%fused_computation.51 | loop fusion | flops 17408 | bytes 24640 | tf_op jit(solution)/shard_map/mul | solution.py:24
  6.4 1.2 %fusion.2 = f32[4,16,64]{2,0,1:T(4,128)S(1)} fusion(f32[16,64,16]{1,2,0:T(8,128)} %param.26, f32[16,64,16]{1,2,0:T(8,128)} %param.27, f32[16,64]{1,0:T(8,128)S(1)} %get-tuple-element.21, f32[16,64]{1,0:T(8,128)S(1)} %get-tuple-element.20, f32[4,16,64]{2,1,0:T(8,128)} %param.32, f32[4,16,64]{2,1,0:T(8,128)} %param.31, f32[16,64]{1,0:T(8,128)S(1)} %get-tuple-element.22, ...), kind=kOutput, calls=%fused_computation.6 | convolution fusion | flops 851968 | bytes 198656 | tf_op jit(solution)/shard_map/sgp,gnp->sgn/dot_general | solution.py:55
  7.6 1.2 %fusion.3 = f32[4,16,64]{2,0,1:T(4,128)S(1)} fusion(f32[16,64,16]{1,2,0:T(8,128)} %param.27, f32[16,64,16]{1,2,0:T(8,128)} %param.26, f32[16,64]{1,0:T(8,128)S(1)} %get-tuple-element.21, f32[16,64]{1,0:T(8,128)S(1)} %get-tuple-element.20, f32[4,16,64]{2,1,0:T(8,128)} %param.32, f32[4,16,64]{2,1,0:T(8,128)} %param.31, f32[16,64]{1,0:T(8,128)S(1)} %get-tuple-element.22, ...), kind=kOutput, calls=%fused_computation.8 | convolution fusion | flops 851968 | bytes 198656 | tf_op jit(solution)/shard_map/sgp,gnp->sgn/dot_general | solution.py:54
  9.0 0.7 %convert_element_type.80 = f32[2048]{0:T(1024)S(1)} convert(bf16[2048]{0:T(1024)(128)(2,1)} %param.34) | non-fusion elementwise | flops 2048 | bytes 12288 | tf_op jit(solution)/shard_map/convert_element_type | solution.py:15
  9.7 1.2 %fusion.60 = f32[16,4,16]{2,1,0:T(4,128)S(1)} fusion(f32[4,16,64]{2,0,1:T(4,128)S(1)} %fusion.3, f32[16,16,64]{2,1,0:T(8,128)} %param.28), kind=kOutput, calls=%fused_computation.84 | convolution fusion | flops 786432 | bytes 86016 | tf_op jit(solution)/shard_map/sgn,gpn->sgp/dot_general | solution.py:58
  10.9 1.2 %fusion.1 = f32[4,16,16]{2,0,1:T(4,128)S(1)} fusion(f32[16,4,16]{2,1,0:T(4,128)S(1)} %fusion.60, f32[4,16,64]{2,0,1:T(4,128)S(1)} %fusion.2, f32[16,16,64]{2,1,0:T(8,128)} %param.29), kind=kOutput, calls=%fused_computation.4 | convolution fusion | flops 787456 | bytes 90112 | tf_op jit(solution)/shard_map/sgn,gpn->sgp/dot_general | solution.py:58
  12.2 0.9 %fusion.46 = f32[4,2048]{1,0:T(4,128)S(1)} fusion(bf16[256,2048]{1,0:T(8,128)(2,1)S(1)} %copy-done, f32[4,256]{1,0:T(4,128)S(1)} %reshape.81, bf16[4,256]{1,0:T(4,128)(2,1)S(1)} %convolution_convert_fusion.2, f32[256]{0:T(256)} %param.30), kind=kOutput, calls=%fused_computation.69 | convolution fusion | flops 4206592 | bytes 1088512 | tf_op jit(solution)/shard_map/dot_general | solution.py:115
  13.2 12.9 %psum.7 = f32[4,2048]{1,0:T(4,128)S(1)} all-reduce(f32[4,2048]{1,0:T(4,128)S(1)} %fusion.46), channel_id=1, replica_groups=mesh['ep'=8,'tp'=4] {'tp'}, use_global_device_ids=true, to_apply=%region_1.0 | all-reduce | flops 8192 | bytes 65536 | tf_op jit(solution)/shard_map/psum | solution.py:115
  26.1 0.9 %fusion.16 = (f32[4]{0:T(128)S(1)}, bf16[4,2048]{1,0:T(4,128)(2,1)S(1)}) fusion(f32[4,2048]{1,0:T(4,128)S(1)} %psum.7, bf16[4,2048]{1,0:T(4,128)(2,1)} %param.20), kind=kLoop, calls=%fused_computation.29 | loop fusion | flops 49148 | bytes 65552 | tf_op jit(solution)/shard_map/reduce_sum | solution.py:14
  26.9 0.8 %select_reduce_fusion.1 = (f32[4,8,2]{1,0,2:T(4,128)S(1)}, bf16[4,8,2]{1,0,2:T(4,128)(2,1)S(1)}) fusion(f32[4,2]{0,1:T(2,128)} %param.36, s32[4,2,8]{2,0,1:T(4,128)S(1)} %copy.74, pred[4,2,8]{2,0,1:T(4,128)(4,1)S(1)} %copy.75), kind=kLoop, calls=%fused_computation.45 | loop fusion | flops 640 | bytes 736 | tf_op jit(solution)/shard_map/reduce_sum | solution.py:72
  28.0 12.5 %all_to_all.15 = bf16[8,2,2048]{2,1,0:T(2,128)(2,1)S(1)} all-to-all(bf16[8,2,2048]{2,1,0:T(2,128)(2,1)S(1)} %copy.76), channel_id=1, replica_groups=mesh['ep'=8,'tp'=4] {'ep'}, dimensions={0} | all-to-all | bytes 131072 | tf_op jit(solution)/shard_map/all_to_all | solution.py:128
  40.6 4.7 %fusion.61 = f32[16,2048]{1,0:T(8,128)S(1)} fusion(bf16[16,2048]{1,0:T(8,128)(2,1)S(1)} %reshape.82, bf16[2048,2048]{1,0:T(8,128)(2,1)} %param.37), kind=kOutput, calls=%fused_computation.85 | convolution fusion | flops 134217728 | bytes 8585216 | tf_op jit(solution)/shard_map/dot_general | solution.py:132
  45.3 1.0 %copy-done.1 = bf16[2048,2048]{1,0:T(8,128)(2,1)S(1)} copy-done((bf16[2048,2048]{1,0:T(8,128)(2,1)S(1)}, bf16[2048,2048]{1,0:T(8,128)(2,1)}, u32[]{:S(2)}) %copy-start.1) | copy-done | bytes 8388632
  46.3 1.2 %fusion = bf16[16,2048]{1,0:T(8,128)(2,1)S(1)} fusion(bf16[16,2048]{1,0:T(8,128)(2,1)S(1)} %reshape.82, bf16[2048,2048]{1,0:T(8,128)(2,1)S(1)} %copy-done.1, f32[16,2048]{1,0:T(8,128)S(1)} %fusion.61), kind=kOutput, calls=%fused_computation.2 | convolution fusion | flops 134414336 | bytes 8650752 | tf_op jit(solution)/shard_map/dot_general | solution.py:133
  47.5 8.5 %all_to_all.16 = bf16[4,16,2048]{2,1,0:T(8,128)(2,1)S(1)} all-to-all(bf16[4,16,2048]{2,1,0:T(8,128)(2,1)S(1)} %stack.2), channel_id=1, replica_groups=mesh['ep'=8,'tp'=4] {'tp'}, dimensions={0} | all-to-all | bytes 524288 | tf_op jit(solution)/shard_map/all_to_all | solution.py:138
  56.1 1.2 %convolution_convert_fusion.1 = bf16[16,512]{1,0:T(8,128)(2,1)S(1)} fusion(bf16[16,8192]{1,0:T(8,128)(2,1)S(1)} %bitcast.43, bf16[8192,512]{1,0:T(8,128)(2,1)S(1)} %bitcast.42), kind=kOutput, calls=%fused_computation.9 | convolution fusion | flops 134225920 | bytes 8667136 | tf_op jit(solution)/shard_map/dot_general | solution.py:136
  57.9 3.3 %all-to-all-start.2 = ((bf16[8,2,512]{2,1,0:T(2,128)(2,1)}), bf16[8,2,512]{2,1,0:T(2,128)(2,1)S(1)}, u32[]{:S(2)}, u32[]{:S(2)}) async-start(bf16[8,2,512]{2,1,0:T(2,128)(2,1)} %reshape.85), calls=%async_computation.2 | async-start | bytes 32768 | tf_op jit(solution)/shard_map/all_to_all | solution.py:144
  62.5 5.3 %all-to-all-done.2 = bf16[8,2,512]{2,1,0:T(2,128)(2,1)S(1)} async-done(((bf16[8,2,512]{2,1,0:T(2,128)(2,1)}), bf16[8,2,512]{2,1,0:T(2,128)(2,1)S(1)}, u32[]{:S(2)}, u32[]{:S(2)}) %all-to-all-start.2) | async-done | bytes 16416 | tf_op jit(solution)/shard_map/all_to_all | solution.py:144
  67.8 0.8 %fusion.5 = bf16[4,512]{1,0:T(4,128)(2,1)} fusion(bf16[8,2,512]{2,1,0:T(2,128)(2,1)S(1)} %all-to-all-done.2, f32[4,8,2]{1,0,2:T(4,128)S(1)} %get-tuple-element.15, bf16[4,2048]{1,0:T(4,128)(2,1)S(1)} %get-tuple-element.18, s32[]{:T(128)S(6)} %select_n.13), kind=kOutput, calls=%fused_computation.12 | convolution fusion | flops 399360 | bytes 24836 | tf_op jit(solution)/shard_map/xcs,xcd->sd/dot_general | solution.py:149
  (29 shorter events, 2.9 us)
Async XLA Ops:
  0.6 11.6 %copy-start = (bf16[256,2048]{1,0:T(8,128)(2,1)S(1)}, bf16[256,2048]{1,0:T(8,128)(2,1)}, u32[]{:S(2)}) copy-start(bf16[256,2048]{1,0:T(8,128)(2,1)} %param.33) | copy-start | bytes 3145732
  40.5 5.8 %copy-start.1 = (bf16[2048,2048]{1,0:T(8,128)(2,1)S(1)}, bf16[2048,2048]{1,0:T(8,128)(2,1)}, u32[]{:S(2)}) copy-start(bf16[2048,2048]{1,0:T(8,128)(2,1)} %param.38) | copy-start | bytes 25165828
  40.6 15.5 %slice-start = ((s8[8388608]{0:T(1024)(128)(4,1)}), s8[4194304]{0:T(1024)(128)(4,1)S(1)}, s32[]{:S(2)}) async-start(s8[8388608]{0:T(1024)(128)(4,1)} %bitcast.41), calls=%async_computation.3 | async-start | bytes 8388608
  46.3 9.8 %slice-start.1 = ((s8[8388608]{0:T(1024)(128)(4,1)}), s8[4194304]{0:T(1024)(128)(4,1)S(1)}, s32[]{:S(2)}) async-start(s8[8388608]{0:T(1024)(128)(4,1)} %bitcast.41), calls=%async_computation.4 | async-start | bytes 8388608
  57.9 9.9 %all-to-all-start.2 = ((bf16[8,2,512]{2,1,0:T(2,128)(2,1)}), bf16[8,2,512]{2,1,0:T(2,128)(2,1)S(1)}, u32[]{:S(2)}, u32[]{:S(2)}) async-start(bf16[8,2,512]{2,1,0:T(2,128)(2,1)} %reshape.85), calls=%async_computation.2 | async-start | bytes 32768 | tf_op jit(solution)/shard_map/all_to_all | solution.py:144
